TPU v7x, 256 devices: a 4x2x16 block of a 4x16x16 slice. The times are simulated.
256 devices in a mesh: grp: 2 (over y), sp: 32 (over z, core), tp: 4 (over x).
Axes of the slice: x: 4, y: 2, z: 16, core: 2. Of those that a mesh axis runs over, the one named last changes fastest.
The devices are a block of a 4x16x16 slice.
Arguments:
- gate_in: bfloat16 [32768, 1536], P(('grp', 'sp'), 'tp'), parts along dimension 0, may hold values from -6 to 6
- mult_in: bfloat16 [32768, 1536], P(('grp', 'sp'), 'tp'), parts along dimension 0, may hold values from -6 to 6
- value_in: bfloat16 [32768, 1536], P(('grp', 'sp'), 'tp'), parts along dimension 0, may hold values from -6 to 6
- doc_ids: int32 [32768], P(('grp', 'sp')), parts along dimension 0, may hold values from 0 to 15, never falling along the last dimension, each value on 1 to 1536 neighbouring positions
- conv_taps: bfloat16 [3, 1536], P(None, 'tp'), may hold values from -3 to 3
- out_proj: bfloat16 [1536, 2048], P('tp'), may hold values from -0.15625 to 0.15625
- resid: bfloat16 [32768, 2048], P(('grp', 'sp', 'tp')), parts along dimension 0, may hold values from -6 to 6
- norm1_gain: float32 [2048], replicated, may hold values from 0.1 to 1.9
- norm1_bias: float32 [2048], replicated, may hold values from -1.5 to 1.5
- expert_ids: int32 [32768, 2], P(('grp', 'sp', 'tp')), parts along dimension 0, may hold values from 0 to 31, all different within a row; in each aligned block of 128 rows (0 to 127, 128 to 255, ...) at most 10 rows name the same one
- expert_wts: float32 [32768, 2], P(('grp', 'sp', 'tp')), parts along dimension 0, may hold values from 0.1 to 1
- w_gate: bfloat16 [32, 2048, 3072], P('sp', None, 'tp'), may hold values from -0.125 to 0.125
- w_up: bfloat16 [32, 2048, 3072], P('sp', None, 'tp'), may hold values from -0.125 to 0.125
- w_down: bfloat16 [32, 3072, 2048], P('sp', 'tp'), may hold values from -0.21582031 to 0.21582031
- norm2_gain: float32 [2048], replicated, may hold values from 0.1 to 1.9
- norm2_bias: float32 [2048], replicated, may hold values from -1.5 to 1.5
Outputs:
- result: bfloat16 [32768, 2048], P(('grp', 'sp', 'tp')), parts along dimension 0
There are 2 independent parts, one for each index of `grp`. A program takes and returns all parts, laid end to end along the dimension named above; an argument that names none is the same for every part. Nothing has to cross between parts.
Inputs may be any that keep to these rules, and one draw needn't show every extreme that they name: `doc_ids`: never falling along the sequence; each document has 1 to 1536 positions and one has exactly 1536. `expert_ids`: each row names 2 different experts. Among the rows of one device no expert is named more than 10 times, and in some device's rows some expert is named exactly 10 times.
All inputs are finite; a program needn't handle non-finite values.
Results may differ from a plain program's by a relative error of at most 0.0095.
Values may be sent and summed in bfloat16 or wider, within the bound.
No kernel may reach another device: no remote copies, remote signals or barrier semaphores. Data moves between devices by JAX's collectives and lax.ppermute only.
A program may use at most 128 MiB of HBM per device.

v0:
```python
import jax
import jax.numpy as jnp
from jax import lax
from jax.sharding import Mesh
from jax.sharding import PartitionSpec as P

SP = ("sp_0", "sp_1")
GRP_SP = ("grp", "sp_0", "sp_1")
GRP_SP_TP = ("grp", "sp_0", "sp_1", "tp")
SUBLANES = 8
residual_scale = 2.0**0.5
norm_eps = 1e-05


def next_in_sequence(x):
    length = lax.axis_size(SP)
    return lax.ppermute(x, SP, [(i, i + 1) for i in range(length - 1)])


def swapped(x):
    return lax.ppermute(x, "sp_1", [(0, 1), (1, 0)])


def layer_norm(pre, gain, bias):
    center = pre - jnp.mean(pre, axis=-1, keepdims=True)
    spread = jnp.mean(center * center, axis=-1, keepdims=True)
    return center * lax.rsqrt(spread + norm_eps) * gain + bias


def dot(a, b):
    return jnp.dot(a, b, preferred_element_type=jnp.float32)


def chunk_slots(capacity, cores):
    width = SUBLANES // cores
    rest = capacity % width
    sizes = ([rest] if rest else []) + [width] * (capacity // width)
    starts = [sum(sizes[:i]) for i in range(len(sizes))]
    return list(zip(starts, sizes))


def shards(
    gate_in,
    mult_in,
    value_in,
    doc_ids,
    conv_taps,
    out_proj,
    resid,
    norm1_gain,
    norm1_bias,
    expert_ids,
    expert_wts,
    w_gate,
    w_up,
    w_down,
    norm2_gain,
    norm2_bias,
):
    n_tp = lax.axis_size("tp")
    chips = lax.axis_size("sp_0")
    cores = lax.axis_size("sp_1")
    experts = chips * cores
    tok_count, top_count = expert_ids.shape
    width = out_proj.shape[1]
    capacity = 5 * tok_count * top_count // (4 * experts)
    tap_weights = conv_taps.astype(jnp.float32)
    taps = tap_weights.shape[0]
    product = mult_in.astype(jnp.float32) * value_in.astype(jnp.float32)
    docs = doc_ids.astype(jnp.float32)
    row_count, channels = product.shape
    tail_docs = jnp.broadcast_to(docs[row_count - taps + 1 :, None], (taps - 1, channels))
    prev = next_in_sequence(jnp.concatenate([product[row_count - taps + 1 :], tail_docs], axis=0))
    prev_rows, prev_docs = (prev[: taps - 1], prev[taps - 1 :, 0])
    meta = jnp.concatenate([expert_ids.astype(jnp.float32).T, expert_wts.T], axis=0)
    metas = jnp.stack([meta, swapped(meta)])
    ext_rows = jnp.concatenate([prev_rows, product], axis=0)
    ext_docs = jnp.concatenate([prev_docs, docs], axis=0)
    filtered = jnp.zeros_like(product)
    for tap_index in range(taps):
        shifted = ext_rows[tap_index : tap_index + row_count]
        same_doc = (ext_docs[tap_index : tap_index + row_count] == docs)[:, None]
        filtered = filtered + tap_weights[tap_index] * jnp.where(same_doc, shifted, 0.0)
    mixed_heads = (gate_in.astype(jnp.float32) * filtered).astype(jnp.bfloat16)
    partial = dot(mixed_heads, out_proj).astype(jnp.bfloat16)
    partials = lax.all_to_all(
        partial.reshape(n_tp, row_count // n_tp, width), "tp", 0, 0, tiled=True
    )
    mixed = jnp.sum(partials.astype(jnp.float32), axis=0)
    hidden_one = layer_norm(
        residual_scale * resid.astype(jnp.float32) + mixed, norm1_gain, norm1_bias
    ).astype(jnp.bfloat16)
    hidden_both = jnp.concatenate([hidden_one, swapped(hidden_one)], axis=0)
    ids, wts = (metas[:, :top_count], metas[:, top_count:])
    numbers = (jnp.arange(chips) * cores + lax.axis_index("sp_1")).astype(jnp.float32)
    named = ids[:, :, None, :] == numbers[None, None, :, None]
    chosen = jnp.any(named, axis=1)
    weight = jnp.sum(jnp.where(named, wts[:, :, None, :], 0.0), axis=1)
    before = (jnp.arange(tok_count)[:, None] < jnp.arange(tok_count)[None, :]).astype(jnp.bfloat16)
    earlier = dot(chosen.astype(jnp.bfloat16), before)
    slot_of = jnp.where(chosen, earlier, -1.0)

    def selected(start, size, values):
        slots = (start + jnp.arange(size)).astype(jnp.float32)
        hit = slot_of.transpose(1, 0, 2)[:, :, None, None, :] == slots[None, None, :, None, None]
        same = jnp.arange(cores)[:, None] == jnp.arange(cores)[None, :]
        hit = hit & same[None, :, None, :, None]
        picked = jnp.where(hit, values.transpose(1, 0, 2)[:, :, None, None, :], 0.0)
        return picked.reshape(chips * cores * size, cores * tok_count)

    chunks = chunk_slots(capacity, cores)
    ones = jnp.ones_like(weight)
    packed = [
        dot(selected(start, size, ones).astype(jnp.bfloat16), hidden_both)
        .astype(jnp.bfloat16)
        .reshape(chips, cores * size, width)
        for start, size in chunks
    ]
    gathered = []
    for i in range(len(chunks)):
        moved = lax.all_to_all(packed[i], "sp_0", 0, 0, tiled=True)
        rest = tuple(packed[i + 1 :])
        moved, rest = lax.optimization_barrier((moved, rest))
        packed[i + 1 :] = list(rest)
        gathered.append(lax.all_gather(moved.reshape(-1, width), "tp", axis=0, tiled=True))
    scattered = []
    for rows_in in gathered:
        gate_act = dot(rows_in, w_gate[0])
        up_act = dot(rows_in, w_up[0])
        hid = (jax.nn.silu(gate_act) * up_act).astype(jnp.bfloat16)
        piece = dot(hid, w_down[0]).astype(jnp.bfloat16)
        scattered.append(lax.psum_scatter(piece, "tp", scatter_dimension=0, tiled=True))
    total = jnp.zeros((cores * tok_count, width), jnp.float32)
    for i, (start, size) in enumerate(chunks):
        ready = scattered[i].reshape(chips, cores * size, width)
        back = lax.all_to_all(ready, "sp_0", 0, 0, tiled=True).reshape(-1, width)
        factor = selected(start, size, weight)
        high = factor.astype(jnp.bfloat16)
        low = (factor - high.astype(jnp.float32)).astype(jnp.bfloat16)
        total = total + dot(high.T, back) + dot(low.T, back)
    moe = total[:tok_count] + swapped(total[tok_count:])
    return layer_norm(
        residual_scale * hidden_one.astype(jnp.float32) + moe, norm2_gain, norm2_bias
    ).astype(jnp.bfloat16)


def solution(mesh):
    torus = Mesh(
        mesh.devices.reshape(mesh.shape["grp"], -1, 2, mesh.shape["tp"]),
        ("grp", "sp_0", "sp_1", "tp"),
    )
    in_specs = (
        P(GRP_SP, "tp"),
        P(GRP_SP, "tp"),
        P(GRP_SP, "tp"),
        P(GRP_SP),
        P(None, "tp"),
        P("tp", None),
        P(GRP_SP_TP, None),
        P(),
        P(),
        P(GRP_SP_TP, None),
        P(GRP_SP_TP, None),
        P(SP, None, "tp"),
        P(SP, None, "tp"),
        P(SP, "tp", None),
        P(),
        P(),
    )
    out_specs = P(GRP_SP_TP, None)
    return jax.shard_map(
        shards, mesh=torus, in_specs=in_specs, out_specs=out_specs, check_vma=False
    )
```

profile of v0, /device:TPU:33, one launch (start us, length us, event | category | flops | bytes accessed | tf_op | source)
XLA Modules:
  0.0 383.8 jit_solution(6780999300419874182)
XLA Ops:
  8.9 5.7 %collective-permute-start = (f32[4,384]{1,0:T(4,128)S(1)}, f32[4,384]{1,0:T(4,128)S(1)}, u32[]{:S(2)}, u32[]{:S(2)}) collective-permute-start(f32[4,384]{1,0:T(4,128)S(1)} %pad_maximum_fusion.5), channel_id=1, source_target_pairs={{0,4},{4,8},{8,12},{12,16},{16,20},{20,24},{24,28},{28,32},{32,36}... | collective-permute-start | bytes 18440 | tf_op jit(solution)/shard_map/ppermute | solution.py:17
  15.3 15.9 %collective-permute-done = f32[4,384]{1,0:T(4,128)S(1)} collective-permute-done((f32[4,384]{1,0:T(4,128)S(1)}, f32[4,384]{1,0:T(4,128)S(1)}, u32[]{:S(2)}, u32[]{:S(2)}) %collective-permute-start) | collective-permute-done | bytes 6176 | tf_op jit(solution)/shard_map/ppermute | solution.py:17
  32.2 4.4 %convolution_convert_fusion = bf16[512,2048]{1,0:T(8,128)(2,1)} fusion(bf16[384,2048]{1,0:T(8,128)(2,1)} %param.21, f32[2,384]{1,0:T(2,128)S(1)} %slice.63, f32[512,384]{1,0:T(8,128)S(1)} %convert_multiply_fusion, bf16[512,384]{1,0:T(8,128)(2,1)} %param.16, f32[384]{0:T(512)S(1)} %get-tuple-element.16, f32[384]{0:T(512)S(1)} %get-tuple-element.17, ...), kind=kOutput, calls=%fused_computation.21 | convolution fusion | flops 808910848 | bytes 4858880 | tf_op jit(solution)/shard_map/dot_general | solution.py:31
  36.6 4.7 %all-to-all-start = ((bf16[4,128,2048]{2,1,0:T(8,128)(2,1)}), bf16[4,128,2048]{2,1,0:T(8,128)(2,1)}, u32[]{:S(2)}, u32[]{:S(2)}) async-start(bf16[4,128,2048]{2,1,0:T(8,128)(2,1)} %bitcast.127), calls=%async_computation | async-start | bytes 4194304 | tf_op jit(solution)/shard_map/all_to_all | solution.py:86
  42.8 24.7 %all-to-all-done = bf16[4,128,2048]{2,1,0:T(8,128)(2,1)} async-done(((bf16[4,128,2048]{2,1,0:T(8,128)(2,1)}), bf16[4,128,2048]{2,1,0:T(8,128)(2,1)}, u32[]{:S(2)}, u32[]{:S(2)}) %all-to-all-start) | async-done | bytes 2097184 | tf_op jit(solution)/shard_map/all_to_all | solution.py:86
  67.5 2.1 convert_reduce_fusion
  75.3 6.6 %all-to-all-start.1 = ((bf16[16,4,2048]{2,1,0:T(4,128)(2,1)}), bf16[16,4,2048]{2,1,0:T(4,128)(2,1)S(1)}, u32[]{:S(2)}, u32[]{:S(2)}) async-start(bf16[16,4,2048]{2,1,0:T(4,128)(2,1)} %reshape.246), calls=%async_computation.1 | async-start | bytes 524288 | tf_op jit(solution)/shard_map/all_to_all | solution.py:121
  83.8 2.3 fusion.31
  87.3 8.4 %all-to-all-done.1 = bf16[16,4,2048]{2,1,0:T(4,128)(2,1)S(1)} async-done(((bf16[16,4,2048]{2,1,0:T(4,128)(2,1)}), bf16[16,4,2048]{2,1,0:T(4,128)(2,1)S(1)}, u32[]{:S(2)}, u32[]{:S(2)}) %all-to-all-start.1) | async-done | bytes 262176 | tf_op jit(solution)/shard_map/all_to_all | solution.py:121
  95.7 10.4 %all-to-all-start.3 = ((bf16[16,8,2048]{2,1,0:T(8,128)(2,1)}), bf16[16,8,2048]{2,1,0:T(8,128)(2,1)}, u32[]{:S(2)}, u32[]{:S(2)}) async-start(bf16[16,8,2048]{2,1,0:T(8,128)(2,1)} %fusion.31), calls=%async_computation.4 | async-start | bytes 1048576 | tf_op jit(solution)/shard_map/all_to_all | solution.py:121
  107.1 21.9 %all-to-all-done.3 = bf16[16,8,2048]{2,1,0:T(8,128)(2,1)} async-done(((bf16[16,8,2048]{2,1,0:T(8,128)(2,1)}), bf16[16,8,2048]{2,1,0:T(8,128)(2,1)}, u32[]{:S(2)}, u32[]{:S(2)}) %all-to-all-start.3) | async-done | bytes 524320 | tf_op jit(solution)/shard_map/all_to_all | solution.py:121
  129.1 35.6 %all_to_all.35 = bf16[16,8,2048]{2,1,0:T(8,128)(2,1)} all-to-all(bf16[16,8,2048]{2,1,0:T(8,128)(2,1)} %fusion.32), channel_id=1, replica_groups=mesh['grp'=2,'sp_0'=16,'sp_1'=2,'tp'=4] {'sp_0'}, dimensions={0} | all-to-all | bytes 1048576 | tf_op jit(solution)/shard_map/all_to_all | solution.py:121
  164.9 4.1 %fusion.16 = f32[256,768]{1,0:T(8,128)} fusion(bf16[256,2048]{1,0:T(8,128)(2,1)} %all-gather.4.cloned.1.call-done, bf16[1,2048,768]{2,1,0:T(8,128)(2,1)} %param.27), kind=kOutput, calls=%fused_computation.17 | convolution fusion | flops 805306368 | bytes 4980736 | tf_op jit(solution)/shard_map/dot_general | solution.py:31
  169.0 5.6 %fusion.28 = bf16[256,2048]{1,0:T(8,128)(2,1)} fusion(bf16[1,768,2048]{2,1,0:T(8,128)(2,1)S(1)} %copy-done, bf16[256,2048]{1,0:T(8,128)(2,1)} %all-gather.4.cloned.1.call-done, bf16[1,2048,768]{2,1,0:T(8,128)(2,1)} %param.28, f32[256,768]{1,0:T(8,128)} %fusion.16), kind=kOutput, calls=%fused_computation.27 | convolution fusion | flops 1612316672 | bytes 9175040 | tf_op jit(solution)/shard_map/dot_general | solution.py:31
  174.9 3.0 all-gather.6.cloned.1.call-done
  177.9 5.5 %fusion.14 = f32[512,768]{1,0:T(8,128)} fusion(bf16[512,2048]{1,0:T(8,128)(2,1)} %all-gather.6.cloned.1.call-done, bf16[1,2048,768]{2,1,0:T(8,128)(2,1)} %param.27), kind=kOutput, calls=%fused_computation.15 | convolution fusion | flops 1610612736 | bytes 6815744 | tf_op jit(solution)/shard_map/dot_general | solution.py:31
  183.3 8.2 %fusion.18 = bf16[512,2048]{1,0:T(8,128)(2,1)} fusion(bf16[1,768,2048]{2,1,0:T(8,128)(2,1)S(1)} %copy-done, f32[512,768]{1,0:T(8,128)} %fusion.14, bf16[512,2048]{1,0:T(8,128)(2,1)} %all-gather.6.cloned.1.call-done, bf16[1,2048,768]{2,1,0:T(8,128)(2,1)} %param.28), kind=kOutput, calls=%fused_computation.19 | convolution fusion | flops 3224633344 | bytes 12058624 | tf_op jit(solution)/shard_map/dot_general | solution.py:31
  191.7 24.9 %all-gather.8.cloned.1.call-done = bf16[512,2048]{1,0:T(8,128)(2,1)} async-done(((bf16[128,2048]{1,0:T(8,128)(2,1)}), bf16[512,2048]{1,0:T(8,128)(2,1)}) %all-gather.8.cloned.1.call-update) | async-done | bytes 2097168 | tf_op jit(solution)/shard_map/all_gather | solution.py:125
  216.7 5.5 %fusion.12 = f32[512,768]{1,0:T(8,128)} fusion(bf16[512,2048]{1,0:T(8,128)(2,1)} %all-gather.8.cloned.1.call-done, bf16[1,2048,768]{2,1,0:T(8,128)(2,1)} %param.27), kind=kOutput, calls=%fused_computation.13 | convolution fusion | flops 1610612736 | bytes 6815744 | tf_op jit(solution)/shard_map/dot_general | solution.py:31
  222.1 8.3 %fusion.21 = bf16[512,2048]{1,0:T(8,128)(2,1)} fusion(bf16[1,768,2048]{2,1,0:T(8,128)(2,1)S(1)} %copy-done, f32[512,768]{1,0:T(8,128)} %fusion.12, bf16[512,2048]{1,0:T(8,128)(2,1)} %all-gather.8.cloned.1.call-done, bf16[1,2048,768]{2,1,0:T(8,128)(2,1)} %param.28), kind=kOutput, calls=%fused_computation.20 | convolution fusion | flops 3224633344 | bytes 12058624 | tf_op jit(solution)/shard_map/dot_general | solution.py:31
  230.5 17.2 %reduce-scatter.4.cloned.1.call-done = bf16[64,2048]{1,0:T(8,128)(2,1)} async-done(((bf16[256,2048]{1,0:T(8,128)(2,1)}), bf16[64,2048]{1,0:T(8,128)(2,1)}) %reduce-scatter.4.cloned.1.call-update) | async-done | bytes 262160 | tf_op jit(solution)/shard_map/reduce_scatter | solution.py:132
  248.7 24.5 %all_to_all.36 = bf16[16,4,2048]{2,1,0:T(4,128)(2,1)} all-to-all(bf16[16,4,2048]{2,1,0:T(4,128)(2,1)S(1)} %reshape.250), channel_id=1, replica_groups=mesh['grp'=2,'sp_0'=16,'sp_1'=2,'tp'=4] {'sp_0'}, dimensions={0} | all-to-all | bytes 524288 | tf_op jit(solution)/shard_map/all_to_all | solution.py:136
  273.3 13.8 %reduce-scatter.6.cloned.1.call-done = bf16[128,2048]{1,0:T(8,128)(2,1)} async-done(((bf16[512,2048]{1,0:T(8,128)(2,1)}), bf16[128,2048]{1,0:T(8,128)(2,1)}) %reduce-scatter.6.cloned.1.call-update) | async-done | bytes 524304 | tf_op jit(solution)/shard_map/reduce_scatter | solution.py:132
  287.0 35.0 %all_to_all.37 = bf16[16,8,2048]{2,1,0:T(8,128)(2,1)} all-to-all(bf16[16,8,2048]{2,1,0:T(8,128)(2,1)} %bitcast.130), channel_id=1, replica_groups=mesh['grp'=2,'sp_0'=16,'sp_1'=2,'tp'=4] {'sp_0'}, dimensions={0} | all-to-all | bytes 1048576 | tf_op jit(solution)/shard_map/all_to_all | solution.py:136
  322.0 3.0 reduce-scatter.8.cloned.1.call-done
  325.0 12.1 %all-to-all-start.6 = ((bf16[16,8,2048]{2,1,0:T(8,128)(2,1)}), bf16[16,8,2048]{2,1,0:T(8,128)(2,1)}, u32[]{:S(2)}, u32[]{:S(2)}) async-start(bf16[16,8,2048]{2,1,0:T(8,128)(2,1)} %bitcast.129), calls=%async_computation.9 | async-start | bytes 1048576 | tf_op jit(solution)/shard_map/all_to_all | solution.py:136
  338.9 2.6 fusion.109
  343.3 1.8 fusion.66
  345.1 14.9 %all-to-all-done.6 = bf16[16,8,2048]{2,1,0:T(8,128)(2,1)} async-done(((bf16[16,8,2048]{2,1,0:T(8,128)(2,1)}), bf16[16,8,2048]{2,1,0:T(8,128)(2,1)}, u32[]{:S(2)}, u32[]{:S(2)}) %all-to-all-start.6) | async-done | bytes 524320 | tf_op jit(solution)/shard_map/all_to_all | solution.py:136
  363.2 2.5 fusion.27
  365.8 7.2 %collective-permute-start.3 = (f32[128,2048]{1,0:T(8,128)S(1)}, f32[128,2048]{1,0:T(8,128)S(1)}, u32[]{:S(2)}, u32[]{:S(2)}) collective-permute-start(f32[128,2048]{1,0:T(8,128)S(1)} %slice.71), channel_id=1, source_target_pairs={{0,4},{4,0},{1,5},{5,1},{2,6},{6,2},{3,7},{7,3},{8,12},{12,8},{9,1... | collective-permute-start | bytes 3145736 | tf_op jit(solution)/shard_map/ppermute | solution.py:21
  373.0 2.3 collective-permute-done.3
  (112 shorter events, 25.1 us)
Async XLA Ops:
  6.5 162.5 %copy-start = (bf16[1,768,2048]{2,1,0:T(8,128)(2,1)S(1)}, bf16[1,768,2048]{2,1,0:T(8,128)(2,1)}, u32[]{:S(2)}) copy-start(bf16[1,768,2048]{2,1,0:T(8,128)(2,1)} %param.29) | copy-start | bytes 9437188
  8.9 22.4 %collective-permute-start = (f32[4,384]{1,0:T(4,128)S(1)}, f32[4,384]{1,0:T(4,128)S(1)}, u32[]{:S(2)}, u32[]{:S(2)}) collective-permute-start(f32[4,384]{1,0:T(4,128)S(1)} %pad_maximum_fusion.5), channel_id=1, source_target_pairs={{0,4},{4,8},{8,12},{12,16},{16,20},{20,24},{24,28},{28,32},{32,36}... | collective-permute-start | bytes 18440 | tf_op jit(solution)/shard_map/ppermute | solution.py:17
  36.6 4.7 %copy-start.19 = (s32[128,2]{0,1:T(2,128)S(1)}, s32[128,2]{0,1:T(2,128)}, u32[]{:S(2)}) copy-start(s32[128,2]{0,1:T(2,128)} %param.25) | copy-start | bytes 3076
  36.6 4.7 %copy-start.20 = (f32[128,2]{0,1:T(2,128)S(1)}, f32[128,2]{0,1:T(2,128)}, u32[]{:S(2)}) copy-start(f32[128,2]{0,1:T(2,128)} %param.26) | copy-start | bytes 3076
  36.6 30.9 %all-to-all-start = ((bf16[4,128,2048]{2,1,0:T(8,128)(2,1)}), bf16[4,128,2048]{2,1,0:T(8,128)(2,1)}, u32[]{:S(2)}, u32[]{:S(2)}) async-start(bf16[4,128,2048]{2,1,0:T(8,128)(2,1)} %bitcast.127), calls=%async_computation | async-start | bytes 4194304 | tf_op jit(solution)/shard_map/all_to_all | solution.py:86
  41.3 1.3 collective-permute-start.1
  41.6 30.5 %copy-start.17 = (pred[2,2]{1,0:T(4,128)(4,1)}, pred[2,2]{1,0:T(4,128)(4,1)S(1)}, u32[]{:S(2)}) copy-start(pred[2,2]{1,0:T(4,128)(4,1)S(1)} %iota_compare_fusion.1) | copy-start | bytes 16
  70.7 2.7 copy-start.5
  70.7 2.7 collective-permute-start.2
  75.3 20.4 %all-to-all-start.1 = ((bf16[16,4,2048]{2,1,0:T(4,128)(2,1)}), bf16[16,4,2048]{2,1,0:T(4,128)(2,1)S(1)}, u32[]{:S(2)}, u32[]{:S(2)}) async-start(bf16[16,4,2048]{2,1,0:T(4,128)(2,1)} %reshape.246), calls=%async_computation.1 | async-start | bytes 524288 | tf_op jit(solution)/shard_map/all_to_all | solution.py:121
  81.9 4.3 %copy-start.6 = (bf16[128,2048]{1,0:T(8,128)(2,1)S(1)}, bf16[128,2048]{1,0:T(8,128)(2,1)}, u32[]{:S(2)}) copy-start(bf16[128,2048]{1,0:T(8,128)(2,1)} %copy-done.5) | copy-start | bytes 1572868
  81.9 4.2 %copy-start.22 = (bf16[128,2048]{1,0:T(8,128)(2,1)S(1)}, bf16[128,2048]{1,0:T(8,128)(2,1)}, u32[]{:S(2)}) copy-start(bf16[128,2048]{1,0:T(8,128)(2,1)} %copy-done.21) | copy-start | bytes 1572868
  95.7 33.3 %all-to-all-start.3 = ((bf16[16,8,2048]{2,1,0:T(8,128)(2,1)}), bf16[16,8,2048]{2,1,0:T(8,128)(2,1)}, u32[]{:S(2)}, u32[]{:S(2)}) async-start(bf16[16,8,2048]{2,1,0:T(8,128)(2,1)} %fusion.31), calls=%async_computation.4 | async-start | bytes 1048576 | tf_op jit(solution)/shard_map/all_to_all | solution.py:121
  106.2 58.7 %all-gather.4.cloned.1.call-start = ((), (), s32[]{:S(2)}) async-start(), calls=%async_computation.10 | async-start | bytes 1310720 | tf_op jit(solution)/shard_map/all_gather | solution.py:125
  107.1 70.8 %all-gather.6.cloned.1.call-start = ((), (), s32[]{:S(2)}) async-start(), calls=%async_computation.12 | async-start | bytes 2621440 | tf_op jit(solution)/shard_map/all_gather | solution.py:125
  129.1 87.6 %all-gather.8.cloned.1.call-start = ((), (), s32[]{:S(2)}) async-start(), calls=%async_computation.14 | async-start | bytes 2621440 | tf_op jit(solution)/shard_map/all_gather | solution.py:125
  164.8 82.9 %reduce-scatter.4.cloned.1.call-start = ((), (), s32[]{:S(2)}) async-start(), calls=%async_computation.11 | async-start | bytes 1310720 | tf_op jit(solution)/shard_map/reduce_scatter | solution.py:132
  174.7 112.3 %reduce-scatter.6.cloned.1.call-start = ((), (), s32[]{:S(2)}) async-start(), calls=%async_computation.13 | async-start | bytes 2621440 | tf_op jit(solution)/shard_map/reduce_scatter | solution.py:132
  191.7 133.4 %reduce-scatter.8.cloned.1.call-start = ((), (), s32[]{:S(2)}) async-start(), calls=%async_computation.15 | async-start | bytes 2621440 | tf_op jit(solution)/shard_map/reduce_scatter | solution.py:132
  273.3 63.9 %copy-start.11 = (pred[16,2,2,128]{3,2,1,0:T(4,128)(4,1)S(1)}, pred[16,2,2,128]{3,2,1,0:T(4,128)(4,1)}, u32[]{:S(2)}) copy-start(pred[16,2,2,128]{3,2,1,0:T(4,128)(4,1)} %copy-done.10) | copy-start | bytes 24580
  273.3 63.9 %copy-start.18 = (pred[2,2]{1,0:T(4,128)(4,1)S(1)}, pred[2,2]{1,0:T(4,128)(4,1)}, u32[]{:S(2)}) copy-start(pred[2,2]{1,0:T(4,128)(4,1)} %copy-done.17) | copy-start | bytes 16
  325.0 35.0 %all-to-all-start.6 = ((bf16[16,8,2048]{2,1,0:T(8,128)(2,1)}), bf16[16,8,2048]{2,1,0:T(8,128)(2,1)}, u32[]{:S(2)}, u32[]{:S(2)}) async-start(bf16[16,8,2048]{2,1,0:T(8,128)(2,1)} %bitcast.129), calls=%async_computation.9 | async-start | bytes 1048576 | tf_op jit(solution)/shard_map/all_to_all | solution.py:136
  338.9 2.6 copy-start.4
  338.9 2.6 copy-start.9
  338.9 4.4 %copy-start.8 = (bf16[16,2,4,2,128]{4,3,2,1,0:T(2,128)(2,1)S(1)}, bf16[16,2,4,2,128]{4,3,2,1,0:T(2,128)(2,1)}, u32[]{:S(2)}) copy-start(bf16[16,2,4,2,128]{4,3,2,1,0:T(2,128)(2,1)} %get-tuple-element.21) | copy-start | bytes 196612
  360.0 3.1 copy-start.1
  360.0 3.2 copy-start.2
  360.0 3.2 copy-start.12
  365.7 9.6 %copy-start.7 = (bf16[128,2048]{1,0:T(8,128)(2,1)S(1)}, bf16[128,2048]{1,0:T(8,128)(2,1)}, u32[]{:S(2)}) copy-start(bf16[128,2048]{1,0:T(8,128)(2,1)} %copy-done.5) | copy-start | bytes 1572868
  365.8 10.1 %copy-start.15 = (f32[2048]{0:T(1024)S(1)}, f32[2048]{0:T(1024)}, u32[]{:S(2)}) copy-start(f32[2048]{0:T(1024)} %param.31) | copy-start | bytes 24580
  365.8 10.1 %copy-start.16 = (f32[2048]{0:T(1024)S(1)}, f32[2048]{0:T(1024)}, u32[]{:S(2)}) copy-start(f32[2048]{0:T(1024)} %param.30) | copy-start | bytes 24580
  365.8 9.4 %collective-permute-start.3 = (f32[128,2048]{1,0:T(8,128)S(1)}, f32[128,2048]{1,0:T(8,128)S(1)}, u32[]{:S(2)}, u32[]{:S(2)}) collective-permute-start(f32[128,2048]{1,0:T(8,128)S(1)} %slice.71), channel_id=1, source_target_pairs={{0,4},{4,0},{1,5},{5,1},{2,6},{6,2},{3,7},{7,3},{8,12},{12,8},{9,1... | collective-permute-start | bytes 3145736 | tf_op jit(solution)/shard_map/ppermute | solution.py:21
  (5 other events, 5.7 us)
Sparse Core Ops, SparseCore 0:
  108.8 27.9 all-gather.3
  138.7 39.1 all-gather.5
  179.7 36.8 all-gather.7
  219.1 28.5 reduce-scatter.3
  250.1 36.8 reduce-scatter.5
  289.4 35.5 reduce-scatter.7
where the time goes:
time: 385 us; the launch traced here: 384 us
  waiting for transfers between devices  152 us (39%)
  blocking collectives  95.1 us (25%)
  matrix products  57.3 us (15%)
  starting transfers between devices  48.7 us (13%)
  between operations  13.9 us (4%)
  other arithmetic  11.9 us (3%)
  local copies, waits for them, and re-layouts  5.08 us (1%)
    all_to_all x2, blocking collectives, shards(): back = lax.all_to_all(ready, 'sp_0', 0, 0, tiled=True).reshape(-1, width)  59.5 us
    dot_general x17, matrix products, dot(): return jnp.dot(a, b, preferred_element_type=jnp.float32)  57.3 us
    all_to_all x1, blocking collectives, shards(): moved = lax.all_to_all(packed[i], 'sp_0', 0, 0, tiled=True)  35.6 us
    reduce_scatter x3, waiting for transfers between devices, shards(): lax.psum_scatter(piece, 'tp', scatter_dimension=0, tiled=True)  34 us
    all_to_all x2, waiting for transfers between devices, shards(): moved = lax.all_to_all(packed[i], 'sp_0', 0, 0, tiled=True)  30.3 us
    all_gather x3, waiting for transfers between devices, shards(): lax.all_gather(moved.reshape(-1, width), 'tp', axis=0, tiled=True)  27.9 us
    all_to_all x1, waiting for transfers between devices, shards(): lax.all_to_all(partial.reshape(n_tp, row_count // n_tp, width), 'tp', 0,...  24.7 us
    all_to_all x2, starting transfers between devices, shards(): moved = lax.all_to_all(packed[i], 'sp_0', 0, 0, tiled=True)  17 us
  transfers between devices with their start and end apart: 14, of which 13 were waited for; matrix products, arithmetic and copies ran while one was open for 14% of the time, Pallas kernels for 0%

commit v1 on v0

--- a/solution.py
+++ b/solution.py
@@ -10,6 +10,28 @@
 SUBLANES = 8
 residual_scale = 2.0**0.5
 norm_eps = 1e-05
+
+
+def joined_along(blocks, dim):
+    blocks = jnp.moveaxis(blocks, 0, dim)
+    shape = blocks.shape
+    return blocks.reshape(*shape[:dim], shape[dim] * shape[dim + 1], *shape[dim + 2 :])
+
+
+def gather_around(x, axis, dim):
+    length = lax.axis_size(axis)
+    pairs = [(i, (i + 1) % length) for i in range(length)]
+    back = [(b, a) for a, b in pairs]
+    lower, upper = ([], [])
+    for step in range(length - 1):
+        if step % 2 == 0:
+            lower.append(lax.ppermute(lower[-1] if lower else x, axis, pairs))
+        else:
+            upper.append(lax.ppermute(upper[-1] if upper else x, axis, back))
+    tiles = jnp.stack([*lower[::-1], x, *upper])
+    shift = lax.axis_index(axis) - len(lower)
+    tiles = tiles[(jnp.arange(length) - shift) % length]
+    return joined_along(tiles, dim)
 
 
 def next_in_sequence(x):
@@ -122,7 +144,7 @@
         rest = tuple(packed[i + 1 :])
         moved, rest = lax.optimization_barrier((moved, rest))
         packed[i + 1 :] = list(rest)
-        gathered.append(lax.all_gather(moved.reshape(-1, width), "tp", axis=0, tiled=True))
+        gathered.append(gather_around(moved.reshape(-1, width), "tp", 0))
     scattered = []
     for rows_in in gathered:
         gate_act = dot(rows_in, w_gate[0])

time: 385 us -> 364 us (0.945)
  waiting for transfers between devices: 152 us -> 114 us
  blocking collectives: 95.1 us -> 69.8 us
  starting transfers between devices: 48.7 us -> 71.5 us
  local copies, waits for them, and re-layouts: 5.08 us -> 16.2 us
  other arithmetic: 11.9 us -> 20.5 us
    all_to_all x1 -> x0, blocking collectives: 35.6 us -> none  [shards(): moved = lax.all_to_all(packed[i], 'sp_0', 0, 0, tiled=True)]
    reduce_scatter x3, waiting for transfers between devices: 34 us -> 0.02 us  [shards(): lax.psum_scatter(piece, 'tp', scatter_dimension=0, tiled=True)]
    ppermute x0 -> x9, waiting for transfers between devices: none -> 31.5 us  [the longest x6 31.5 us: gather_around(): lower.append(lax.ppermute(lower[-1] if lower else x, axis, pairs))]
    all_gather x3 -> x0, waiting for transfers between devices: 27.9 us -> none  [shards(): lax.all_gather(moved.reshape(-1, width), 'tp', axis=0, tiled=True)]
    all_to_all x2 -> x3, starting transfers between devices: 17 us -> 32.1 us  [shards(): moved = lax.all_to_all(packed[i], 'sp_0', 0, 0, tiled=True)]
    gather x0 -> x3, local copies, waits for them, and re-layouts: none -> 10.4 us  [gather_around(): tiles = tiles[(jnp.arange(length) - shift) % length]]
    all_to_all x2, blocking collectives: 59.5 us -> 69.8 us  [shards(): back = lax.all_to_all(ready, 'sp_0', 0, 0, tiled=True).reshape(-1, width)]
    ppermute x0 -> x9, starting transfers between devices: none -> 8.04 us  [the longest x3 7.04 us: gather_around(): upper.append(lax.ppermute(upper[-1] if upper else x, axis, back))]
  transfers between devices with their start and end apart: 14 -> 21, of which waited for: 13 -> 12; matrix products, arithmetic and copies ran while one was open for 14% -> 20% of each run, Pallas kernels for 0% -> 0%
where the time goes in v1:
time: 364 us; the launch traced here: 363 us
  waiting for transfers between devices  114 us (31%)
  starting transfers between devices  71.5 us (20%)
  blocking collectives  69.8 us (19%)
  matrix products  57.4 us (16%)
  other arithmetic  20.5 us (6%)
  local copies, waits for them, and re-layouts  16.2 us (4%)
  between operations  13.6 us (4%)
    all_to_all x2, blocking collectives, shards(): back = lax.all_to_all(ready, 'sp_0', 0, 0, tiled=True).reshape(-1, width)  69.8 us
    dot_general x17, matrix products, dot(): return jnp.dot(a, b, preferred_element_type=jnp.float32)  57.4 us
    all_to_all x3, starting transfers between devices, shards(): moved = lax.all_to_all(packed[i], 'sp_0', 0, 0, tiled=True)  32.1 us
    ppermute x6, waiting for transfers between devices, gather_around(): lower.append(lax.ppermute(lower[-1] if lower else x, axis, pairs))  31.5 us
    all_to_all x1, waiting for transfers between devices, shards(): lax.all_to_all(partial.reshape(n_tp, row_count // n_tp, width), 'tp', 0,...  24.7 us
    all_to_all x3, waiting for transfers between devices, shards(): moved = lax.all_to_all(packed[i], 'sp_0', 0, 0, tiled=True)  22.5 us
    ppermute x1, waiting for transfers between devices, next_in_sequence(): return lax.ppermute(x, SP, [(i, i + 1) for i in range(length - 1)])  15.9 us
    all_to_all x1, waiting for transfers between devices, shards(): back = lax.all_to_all(ready, 'sp_0', 0, 0, tiled=True).reshape(-1, width)  15 us
  transfers between devices with their start and end apart: 21, of which 12 were waited for; matrix products, arithmetic and copies ran while one was open for 20% of the time, Pallas kernels for 0%

profile of v1, /device:TPU:33, one launch (start us, length us, event | category | flops | bytes accessed | tf_op | source)
XLA Modules:
  0.0 362.6 jit_solution(16732855878891076886)
XLA Ops:
  8.9 5.7 %collective-permute-start = (f32[4,384]{1,0:T(4,128)S(1)}, f32[4,384]{1,0:T(4,128)S(1)}, u32[]{:S(2)}, u32[]{:S(2)}) collective-permute-start(f32[4,384]{1,0:T(4,128)S(1)} %pad_maximum_fusion.8), channel_id=1, source_target_pairs={{0,4},{4,8},{8,12},{12,16},{16,20},{20,24},{24,28},{28,32},{32,36}... | collective-permute-start | bytes 18440 | tf_op jit(solution)/shard_map/ppermute | solution.py:39
  15.3 15.9 %collective-permute-done = f32[4,384]{1,0:T(4,128)S(1)} collective-permute-done((f32[4,384]{1,0:T(4,128)S(1)}, f32[4,384]{1,0:T(4,128)S(1)}, u32[]{:S(2)}, u32[]{:S(2)}) %collective-permute-start) | collective-permute-done | bytes 6176 | tf_op jit(solution)/shard_map/ppermute | solution.py:39
  32.2 4.4 %convolution_convert_fusion = bf16[512,2048]{1,0:T(8,128)(2,1)} fusion(bf16[384,2048]{1,0:T(8,128)(2,1)} %param.21, f32[2,384]{1,0:T(2,128)S(1)} %slice.69, f32[512,384]{1,0:T(8,128)S(1)} %convert_multiply_fusion, bf16[512,384]{1,0:T(8,128)(2,1)} %param.16, f32[384]{0:T(512)S(1)} %get-tuple-element.16, f32[384]{0:T(512)S(1)} %get-tuple-element.17, ...), kind=kOutput, calls=%fused_computation.24 | convolution fusion | flops 808910848 | bytes 4858880 | tf_op jit(solution)/shard_map/dot_general | solution.py:53
  36.6 4.7 %all-to-all-start = ((bf16[4,128,2048]{2,1,0:T(8,128)(2,1)}), bf16[4,128,2048]{2,1,0:T(8,128)(2,1)}, u32[]{:S(2)}, u32[]{:S(2)}) async-start(bf16[4,128,2048]{2,1,0:T(8,128)(2,1)} %bitcast.143), calls=%async_computation | async-start | bytes 4194304 | tf_op jit(solution)/shard_map/all_to_all | solution.py:108
  42.8 24.7 %all-to-all-done = bf16[4,128,2048]{2,1,0:T(8,128)(2,1)} async-done(((bf16[4,128,2048]{2,1,0:T(8,128)(2,1)}), bf16[4,128,2048]{2,1,0:T(8,128)(2,1)}, u32[]{:S(2)}, u32[]{:S(2)}) %all-to-all-start) | async-done | bytes 2097184 | tf_op jit(solution)/shard_map/all_to_all | solution.py:108
  75.3 6.6 %all-to-all-start.1 = ((bf16[16,4,2048]{2,1,0:T(4,128)(2,1)}), bf16[16,4,2048]{2,1,0:T(4,128)(2,1)S(1)}, u32[]{:S(2)}, u32[]{:S(2)}) async-start(bf16[16,4,2048]{2,1,0:T(4,128)(2,1)} %reshape.304), calls=%async_computation.1 | async-start | bytes 524288 | tf_op jit(solution)/shard_map/all_to_all | solution.py:143
  87.2 8.5 %all-to-all-done.1 = bf16[16,4,2048]{2,1,0:T(4,128)(2,1)S(1)} async-done(((bf16[16,4,2048]{2,1,0:T(4,128)(2,1)}), bf16[16,4,2048]{2,1,0:T(4,128)(2,1)S(1)}, u32[]{:S(2)}, u32[]{:S(2)}) %all-to-all-start.1) | async-done | bytes 262176 | tf_op jit(solution)/shard_map/all_to_all | solution.py:143
  95.7 10.4 %all-to-all-start.3 = ((bf16[16,8,2048]{2,1,0:T(8,128)(2,1)}), bf16[16,8,2048]{2,1,0:T(8,128)(2,1)}, u32[]{:S(2)}, u32[]{:S(2)}) async-start(bf16[16,8,2048]{2,1,0:T(8,128)(2,1)} %fusion.31), calls=%async_computation.4 | async-start | bytes 1048576 | tf_op jit(solution)/shard_map/all_to_all | solution.py:143
  109.6 5.8 %collective-permute-done.3 = bf16[64,2048]{1,0:T(8,128)(2,1)} collective-permute-done((bf16[64,2048]{1,0:T(8,128)(2,1)}, bf16[64,2048]{1,0:T(8,128)(2,1)}, u32[]{:S(2)}, u32[]{:S(2)}) %collective-permute-start.3) | collective-permute-done | bytes 262176 | tf_op jit(solution)/shard_map/ppermute | solution.py:28
  116.8 12.1 %all-to-all-done.3 = bf16[16,8,2048]{2,1,0:T(8,128)(2,1)} async-done(((bf16[16,8,2048]{2,1,0:T(8,128)(2,1)}), bf16[16,8,2048]{2,1,0:T(8,128)(2,1)}, u32[]{:S(2)}, u32[]{:S(2)}) %all-to-all-start.3) | async-done | bytes 524320 | tf_op jit(solution)/shard_map/all_to_all | solution.py:143
  131.8 2.9 gather_fusion
  134.7 4.1 %fusion.16 = f32[256,768]{1,0:T(8,128)} fusion(bf16[256,2048]{1,0:T(8,128)(2,1)} %bitcast.148, bf16[1,2048,768]{2,1,0:T(8,128)(2,1)} %param.27), kind=kOutput, calls=%fused_computation.20 | convolution fusion | flops 805306368 | bytes 4980736 | tf_op jit(solution)/shard_map/dot_general | solution.py:53
  141.0 5.6 %fusion.28 = bf16[256,2048]{1,0:T(8,128)(2,1)} fusion(bf16[1,768,2048]{2,1,0:T(8,128)(2,1)S(1)} %copy-done, bf16[256,2048]{1,0:T(8,128)(2,1)} %bitcast.149, bf16[1,2048,768]{2,1,0:T(8,128)(2,1)} %param.28, f32[256,768]{1,0:T(8,128)} %fusion.16), kind=kOutput, calls=%fused_computation.30 | convolution fusion | flops 1612316672 | bytes 9175040 | tf_op jit(solution)/shard_map/dot_general | solution.py:53
  146.6 15.2 %all-to-all-start.5 = ((bf16[16,8,2048]{2,1,0:T(8,128)(2,1)}), bf16[16,8,2048]{2,1,0:T(8,128)(2,1)}, u32[]{:S(2)}, u32[]{:S(2)}) async-start(bf16[16,8,2048]{2,1,0:T(8,128)(2,1)} %fusion.32), calls=%async_computation.7 | async-start | bytes 1048576 | tf_op jit(solution)/shard_map/all_to_all | solution.py:143
  161.9 3.1 pad_maximum_fusion
  165.0 3.7 %gather_fusion.1 = bf16[4,128,2048]{2,1,0:T(8,128)(2,1)} fusion(bf16[4,128,2048]{2,1,0:T(8,128)(2,1)} %pad_maximum_fusion, s32[1024]{0:T(1024)} %pad_clamp_fusion), kind=kCustom, calls=%fused_computation.1 | custom fusion | bytes 4194320 | tf_op jit(solution)/shard_map/gather | solution.py:33
  168.7 5.5 %fusion.14 = f32[512,768]{1,0:T(8,128)} fusion(bf16[512,2048]{1,0:T(8,128)(2,1)} %bitcast.146, bf16[1,2048,768]{2,1,0:T(8,128)(2,1)} %param.27), kind=kOutput, calls=%fused_computation.18 | convolution fusion | flops 1610612736 | bytes 6815744 | tf_op jit(solution)/shard_map/dot_general | solution.py:53
  174.2 8.3 %fusion.18 = bf16[512,2048]{1,0:T(8,128)(2,1)} fusion(bf16[1,768,2048]{2,1,0:T(8,128)(2,1)S(1)} %copy-done, f32[512,768]{1,0:T(8,128)} %fusion.14, bf16[512,2048]{1,0:T(8,128)(2,1)} %bitcast.147, bf16[1,2048,768]{2,1,0:T(8,128)(2,1)} %param.28), kind=kOutput, calls=%fused_computation.22 | convolution fusion | flops 3224633344 | bytes 12058624 | tf_op jit(solution)/shard_map/dot_general | solution.py:53
  184.5 2.7 collective-permute-start.11
  187.2 6.8 %collective-permute-done.9 = bf16[128,2048]{1,0:T(8,128)(2,1)S(1)} collective-permute-done((bf16[128,2048]{1,0:T(8,128)(2,1)}, bf16[128,2048]{1,0:T(8,128)(2,1)S(1)}, u32[]{:S(2)}, u32[]{:S(2)}) %collective-permute-start.9) | collective-permute-done | bytes 524320 | tf_op jit(solution)/shard_map/ppermute | solution.py:28
  194.0 18.9 %collective-permute-done.10 = bf16[128,2048]{1,0:T(8,128)(2,1)S(1)} collective-permute-done((bf16[128,2048]{1,0:T(8,128)(2,1)S(1)}, bf16[128,2048]{1,0:T(8,128)(2,1)S(1)}, u32[]{:S(2)}, u32[]{:S(2)}) %collective-permute-start.10) | collective-permute-done | bytes 524320 | tf_op jit(solution)/shard_map/ppermute | solution.py:28
  212.9 2.6 pad_maximum_fusion.1
  215.5 3.8 %gather_fusion.2 = bf16[4,128,2048]{2,1,0:T(8,128)(2,1)} fusion(bf16[4,128,2048]{2,1,0:T(8,128)(2,1)} %pad_maximum_fusion.1, s32[1024]{0:T(1024)} %pad_clamp_fusion), kind=kCustom, calls=%fused_computation.2 | custom fusion | bytes 4194320 | tf_op jit(solution)/shard_map/gather | solution.py:33
  219.3 5.5 %fusion.12 = f32[512,768]{1,0:T(8,128)} fusion(bf16[512,2048]{1,0:T(8,128)(2,1)} %bitcast.144, bf16[1,2048,768]{2,1,0:T(8,128)(2,1)} %param.27), kind=kOutput, calls=%fused_computation.16 | convolution fusion | flops 1610612736 | bytes 6815744 | tf_op jit(solution)/shard_map/dot_general | solution.py:53
  224.8 8.3 %fusion.21 = bf16[512,2048]{1,0:T(8,128)(2,1)} fusion(bf16[1,768,2048]{2,1,0:T(8,128)(2,1)S(1)} %copy-done, f32[512,768]{1,0:T(8,128)} %fusion.12, bf16[512,2048]{1,0:T(8,128)(2,1)} %bitcast.145, bf16[1,2048,768]{2,1,0:T(8,128)(2,1)} %param.28), kind=kOutput, calls=%fused_computation.23 | convolution fusion | flops 3224633344 | bytes 12058624 | tf_op jit(solution)/shard_map/dot_general | solution.py:53
  234.2 35.9 %all_to_all.35 = bf16[16,4,2048]{2,1,0:T(4,128)(2,1)} all-to-all(bf16[16,4,2048]{2,1,0:T(4,128)(2,1)S(1)} %reshape.309), channel_id=1, replica_groups=mesh['grp'=2,'sp_0'=16,'sp_1'=2,'tp'=4] {'sp_0'}, dimensions={0} | all-to-all | bytes 524288 | tf_op jit(solution)/shard_map/all_to_all | solution.py:158
  270.1 33.9 %all_to_all.36 = bf16[16,8,2048]{2,1,0:T(8,128)(2,1)} all-to-all(bf16[16,8,2048]{2,1,0:T(8,128)(2,1)} %bitcast.150), channel_id=1, replica_groups=mesh['grp'=2,'sp_0'=16,'sp_1'=2,'tp'=4] {'sp_0'}, dimensions={0} | all-to-all | bytes 1048576 | tf_op jit(solution)/shard_map/all_to_all | solution.py:158
  304.1 12.3 %all-to-all-start.6 = ((bf16[16,8,2048]{2,1,0:T(8,128)(2,1)}), bf16[16,8,2048]{2,1,0:T(8,128)(2,1)}, u32[]{:S(2)}, u32[]{:S(2)}) async-start(bf16[16,8,2048]{2,1,0:T(8,128)(2,1)} %bitcast.151), calls=%async_computation.9 | async-start | bytes 1048576 | tf_op jit(solution)/shard_map/all_to_all | solution.py:158
  318.2 2.6 fusion.109
  324.3 15.0 %all-to-all-done.6 = bf16[16,8,2048]{2,1,0:T(8,128)(2,1)} async-done(((bf16[16,8,2048]{2,1,0:T(8,128)(2,1)}), bf16[16,8,2048]{2,1,0:T(8,128)(2,1)}, u32[]{:S(2)}, u32[]{:S(2)}) %all-to-all-start.6) | async-done | bytes 524320 | tf_op jit(solution)/shard_map/all_to_all | solution.py:158
  342.5 2.5 fusion.27
  345.1 7.0 %collective-permute-start.12 = (f32[128,2048]{1,0:T(8,128)S(1)}, f32[128,2048]{1,0:T(8,128)S(1)}, u32[]{:S(2)}, u32[]{:S(2)}) collective-permute-start(f32[128,2048]{1,0:T(8,128)S(1)} %slice.77), channel_id=1, source_target_pairs={{0,4},{4,0},{1,5},{5,1},{2,6},{6,2},{3,7},{7,3},{8,12},{12,8},{9,1... | collective-permute-start | bytes 3145736 | tf_op jit(solution)/shard_map/ppermute | solution.py:43
  (131 shorter events, 44.1 us)
Async XLA Ops:
  6.5 134.4 %copy-start = (bf16[1,768,2048]{2,1,0:T(8,128)(2,1)S(1)}, bf16[1,768,2048]{2,1,0:T(8,128)(2,1)}, u32[]{:S(2)}) copy-start(bf16[1,768,2048]{2,1,0:T(8,128)(2,1)} %param.29) | copy-start | bytes 9437188
  8.9 22.4 %collective-permute-start = (f32[4,384]{1,0:T(4,128)S(1)}, f32[4,384]{1,0:T(4,128)S(1)}, u32[]{:S(2)}, u32[]{:S(2)}) collective-permute-start(f32[4,384]{1,0:T(4,128)S(1)} %pad_maximum_fusion.8), channel_id=1, source_target_pairs={{0,4},{4,8},{8,12},{12,16},{16,20},{20,24},{24,28},{28,32},{32,36}... | collective-permute-start | bytes 18440 | tf_op jit(solution)/shard_map/ppermute | solution.py:39
  36.6 4.7 %copy-start.19 = (s32[128,2]{0,1:T(2,128)S(1)}, s32[128,2]{0,1:T(2,128)}, u32[]{:S(2)}) copy-start(s32[128,2]{0,1:T(2,128)} %param.25) | copy-start | bytes 3076
  36.6 4.7 %copy-start.20 = (f32[128,2]{0,1:T(2,128)S(1)}, f32[128,2]{0,1:T(2,128)}, u32[]{:S(2)}) copy-start(f32[128,2]{0,1:T(2,128)} %param.26) | copy-start | bytes 3076
  36.6 30.9 %all-to-all-start = ((bf16[4,128,2048]{2,1,0:T(8,128)(2,1)}), bf16[4,128,2048]{2,1,0:T(8,128)(2,1)}, u32[]{:S(2)}, u32[]{:S(2)}) async-start(bf16[4,128,2048]{2,1,0:T(8,128)(2,1)} %bitcast.143), calls=%async_computation | async-start | bytes 4194304 | tf_op jit(solution)/shard_map/all_to_all | solution.py:108
  41.3 1.3 collective-permute-start.1
  41.6 30.5 %copy-start.17 = (pred[2,2]{1,0:T(4,128)(4,1)}, pred[2,2]{1,0:T(4,128)(4,1)S(1)}, u32[]{:S(2)}) copy-start(pred[2,2]{1,0:T(4,128)(4,1)S(1)} %iota_compare_fusion.1) | copy-start | bytes 16
  70.7 2.7 collective-permute-start.2
  75.3 20.4 %all-to-all-start.1 = ((bf16[16,4,2048]{2,1,0:T(4,128)(2,1)}), bf16[16,4,2048]{2,1,0:T(4,128)(2,1)S(1)}, u32[]{:S(2)}, u32[]{:S(2)}) async-start(bf16[16,4,2048]{2,1,0:T(4,128)(2,1)} %reshape.304), calls=%async_computation.1 | async-start | bytes 524288 | tf_op jit(solution)/shard_map/all_to_all | solution.py:143
  81.9 4.2 %copy-start.6 = (bf16[128,2048]{1,0:T(8,128)(2,1)S(1)}, bf16[128,2048]{1,0:T(8,128)(2,1)}, u32[]{:S(2)}) copy-start(bf16[128,2048]{1,0:T(8,128)(2,1)} %copy-done.5) | copy-start | bytes 1572868
  95.7 33.3 %all-to-all-start.3 = ((bf16[16,8,2048]{2,1,0:T(8,128)(2,1)}), bf16[16,8,2048]{2,1,0:T(8,128)(2,1)}, u32[]{:S(2)}, u32[]{:S(2)}) async-start(bf16[16,8,2048]{2,1,0:T(8,128)(2,1)} %fusion.31), calls=%async_computation.4 | async-start | bytes 1048576 | tf_op jit(solution)/shard_map/all_to_all | solution.py:143
  106.1 127.0 %reduce-scatter.4.cloned.1.call-start = ((), (), s32[]{:S(2)}) async-start(), calls=%async_computation.10 | async-start | bytes 1310720 | tf_op jit(solution)/shard_map/reduce_scatter | solution.py:154
  106.9 8.5 %collective-permute-start.3 = (bf16[64,2048]{1,0:T(8,128)(2,1)}, bf16[64,2048]{1,0:T(8,128)(2,1)}, u32[]{:S(2)}, u32[]{:S(2)}) collective-permute-start(bf16[64,2048]{1,0:T(8,128)(2,1)} %reshape.307), channel_id=1, source_target_pairs={{0,1},{1,2},{2,3},{3,0},{4,5},{5,6},{6,7},{7,4},{8,9},{9,10},{10,1... | collective-permute-start | bytes 786440 | tf_op jit(solution)/shard_map/ppermute | solution.py:28
  107.4 22.0 %collective-permute-start.5 = (bf16[64,2048]{1,0:T(8,128)(2,1)}, bf16[64,2048]{1,0:T(8,128)(2,1)}, u32[]{:S(2)}, u32[]{:S(2)}) collective-permute-start(bf16[64,2048]{1,0:T(8,128)(2,1)} %reshape.307), channel_id=1, source_target_pairs={{1,0},{2,1},{3,2},{0,3},{5,4},{6,5},{7,6},{4,7},{9,8},{10,9},{11,1... | collective-permute-start | bytes 786440 | tf_op jit(solution)/shard_map/ppermute | solution.py:30
  115.4 14.0 %collective-permute-start.4 = (bf16[64,2048]{1,0:T(8,128)(2,1)}, bf16[64,2048]{1,0:T(8,128)(2,1)}, u32[]{:S(2)}, u32[]{:S(2)}) collective-permute-start(bf16[64,2048]{1,0:T(8,128)(2,1)} %collective-permute-done.3), channel_id=1, source_target_pairs={{0,1},{1,2},{2,3},{3,0},{4,5},{5,6},{6,7},{7,4},{8,9},{9,10},{10,1... | collective-permute-start | bytes 786440 | tf_op jit(solution)/shard_map/ppermute | solution.py:28
  129.0 12.0 %collective-permute-start.6 = (bf16[128,2048]{1,0:T(8,128)(2,1)}, bf16[128,2048]{1,0:T(8,128)(2,1)}, u32[]{:S(2)}, u32[]{:S(2)}) collective-permute-start(bf16[128,2048]{1,0:T(8,128)(2,1)} %bitcast.18), channel_id=1, source_target_pairs={{0,1},{1,2},{2,3},{3,0},{4,5},{5,6},{6,7},{7,4},{8,9},{9,10},{10,1... | collective-permute-start | bytes 1572872 | tf_op jit(solution)/shard_map/ppermute | solution.py:28
  138.8 23.1 %collective-permute-start.8 = (bf16[128,2048]{1,0:T(8,128)(2,1)}, bf16[128,2048]{1,0:T(8,128)(2,1)}, u32[]{:S(2)}, u32[]{:S(2)}) collective-permute-start(bf16[128,2048]{1,0:T(8,128)(2,1)} %bitcast.18), channel_id=1, source_target_pairs={{1,0},{2,1},{3,2},{0,3},{5,4},{6,5},{7,6},{4,7},{9,8},{10,9},{11,1... | collective-permute-start | bytes 1572872 | tf_op jit(solution)/shard_map/ppermute | solution.py:30
  141.0 20.9 %collective-permute-start.7 = (bf16[128,2048]{1,0:T(8,128)(2,1)}, bf16[128,2048]{1,0:T(8,128)(2,1)}, u32[]{:S(2)}, u32[]{:S(2)}) collective-permute-start(bf16[128,2048]{1,0:T(8,128)(2,1)} %collective-permute-done.6), channel_id=1, source_target_pairs={{0,1},{1,2},{2,3},{3,0},{4,5},{5,6},{6,7},{7,4},{8,9},{9,10},{10,1... | collective-permute-start | bytes 1572872 | tf_op jit(solution)/shard_map/ppermute | solution.py:28
  146.6 37.9 %all-to-all-start.5 = ((bf16[16,8,2048]{2,1,0:T(8,128)(2,1)}), bf16[16,8,2048]{2,1,0:T(8,128)(2,1)}, u32[]{:S(2)}, u32[]{:S(2)}) async-start(bf16[16,8,2048]{2,1,0:T(8,128)(2,1)} %fusion.32), calls=%async_computation.7 | async-start | bytes 1048576 | tf_op jit(solution)/shard_map/all_to_all | solution.py:143
  161.8 108.3 %reduce-scatter.6.cloned.1.call-start = ((), (), s32[]{:S(2)}) async-start(), calls=%async_computation.11 | async-start | bytes 2621440 | tf_op jit(solution)/shard_map/reduce_scatter | solution.py:154
  182.6 121.5 %reduce-scatter.8.cloned.1.call-start = ((), (), s32[]{:S(2)}) async-start(), calls=%async_computation.12 | async-start | bytes 2621440 | tf_op jit(solution)/shard_map/reduce_scatter | solution.py:154
  184.5 9.5 %collective-permute-start.9 = (bf16[128,2048]{1,0:T(8,128)(2,1)}, bf16[128,2048]{1,0:T(8,128)(2,1)S(1)}, u32[]{:S(2)}, u32[]{:S(2)}) collective-permute-start(bf16[128,2048]{1,0:T(8,128)(2,1)} %bitcast.26), channel_id=1, source_target_pairs={{0,1},{1,2},{2,3},{3,0},{4,5},{5,6},{6,7},{7,4},{8,9},{9,10},{10,1... | collective-permute-start | bytes 1572872 | tf_op jit(solution)/shard_map/ppermute | solution.py:28
  184.5 9.5 %collective-permute-start.11 = (bf16[128,2048]{1,0:T(8,128)(2,1)}, bf16[128,2048]{1,0:T(8,128)(2,1)S(1)}, u32[]{:S(2)}, u32[]{:S(2)}) collective-permute-start(bf16[128,2048]{1,0:T(8,128)(2,1)} %bitcast.26), channel_id=1, source_target_pairs={{1,0},{2,1},{3,2},{0,3},{5,4},{6,5},{7,6},{4,7},{9,8},{10,9},{11,1... | collective-permute-start | bytes 1572872 | tf_op jit(solution)/shard_map/ppermute | solution.py:30
  194.0 18.9 %collective-permute-start.10 = (bf16[128,2048]{1,0:T(8,128)(2,1)S(1)}, bf16[128,2048]{1,0:T(8,128)(2,1)S(1)}, u32[]{:S(2)}, u32[]{:S(2)}) collective-permute-start(bf16[128,2048]{1,0:T(8,128)(2,1)S(1)} %collective-permute-done.9), channel_id=1, source_target_pairs={{0,1},{1,2},{2,3},{3,0},{4,5},{5,6},{6,7},{7,4},{8,9},{9,10},{10,1... | collective-permute-start | bytes 1572872 | tf_op jit(solution)/shard_map/ppermute | solution.py:28
  270.1 46.3 %copy-start.11 = (pred[16,2,2,128]{3,2,1,0:T(4,128)(4,1)S(1)}, pred[16,2,2,128]{3,2,1,0:T(4,128)(4,1)}, u32[]{:S(2)}) copy-start(pred[16,2,2,128]{3,2,1,0:T(4,128)(4,1)} %copy-done.10) | copy-start | bytes 24580
  270.1 46.3 %copy-start.18 = (pred[2,2]{1,0:T(4,128)(4,1)S(1)}, pred[2,2]{1,0:T(4,128)(4,1)}, u32[]{:S(2)}) copy-start(pred[2,2]{1,0:T(4,128)(4,1)} %copy-done.17) | copy-start | bytes 16
  304.1 35.3 %all-to-all-start.6 = ((bf16[16,8,2048]{2,1,0:T(8,128)(2,1)}), bf16[16,8,2048]{2,1,0:T(8,128)(2,1)}, u32[]{:S(2)}, u32[]{:S(2)}) async-start(bf16[16,8,2048]{2,1,0:T(8,128)(2,1)} %bitcast.151), calls=%async_computation.9 | async-start | bytes 1048576 | tf_op jit(solution)/shard_map/all_to_all | solution.py:158
  318.2 4.4 %copy-start.8 = (bf16[16,2,4,2,128]{4,3,2,1,0:T(2,128)(2,1)S(1)}, bf16[16,2,4,2,128]{4,3,2,1,0:T(2,128)(2,1)}, u32[]{:S(2)}) copy-start(bf16[16,2,4,2,128]{4,3,2,1,0:T(2,128)(2,1)} %get-tuple-element.21) | copy-start | bytes 196612
  345.0 9.4 %copy-start.7 = (bf16[128,2048]{1,0:T(8,128)(2,1)S(1)}, bf16[128,2048]{1,0:T(8,128)(2,1)}, u32[]{:S(2)}) copy-start(bf16[128,2048]{1,0:T(8,128)(2,1)} %copy-done.5) | copy-start | bytes 1572868
  345.1 9.9 %copy-start.15 = (f32[2048]{0:T(1024)S(1)}, f32[2048]{0:T(1024)}, u32[]{:S(2)}) copy-start(f32[2048]{0:T(1024)} %param.31) | copy-start | bytes 24580
  345.1 9.9 %copy-start.16 = (f32[2048]{0:T(1024)S(1)}, f32[2048]{0:T(1024)}, u32[]{:S(2)}) copy-start(f32[2048]{0:T(1024)} %param.30) | copy-start | bytes 24580
  345.1 9.3 %collective-permute-start.12 = (f32[128,2048]{1,0:T(8,128)S(1)}, f32[128,2048]{1,0:T(8,128)S(1)}, u32[]{:S(2)}, u32[]{:S(2)}) collective-permute-start(f32[128,2048]{1,0:T(8,128)S(1)} %slice.77), channel_id=1, source_target_pairs={{0,4},{4,0},{1,5},{5,1},{2,6},{6,2},{3,7},{7,3},{8,12},{12,8},{9,1... | collective-permute-start | bytes 3145736 | tf_op jit(solution)/shard_map/ppermute | solution.py:43
  (12 other events, 27.3 us)
Sparse Core Ops, SparseCore 0:
  146.7 34.3 reduce-scatter.3
  183.7 47.1 reduce-scatter.5
  233.4 48.4 reduce-scatter.7
